TPU v7x, 32 devices: a whole 2x2x4 slice. The times are simulated.
32 devices in a mesh: ep: 8 (over z, core), tp: 4 (over y, x).
Axes of the slice: x: 2, y: 2, z: 4, core: 2. Of those that a mesh axis runs over, the one named last changes fastest.
Arguments:
- mixer_rows: bfloat16 [4096, 2048], P('ep', 'tp'), may hold values from -6 to 6
- expert_rows: bfloat16 [4096, 2048], P('ep', 'tp'), may hold values from -6 to 6
- mixer_gain: float32 [2048], replicated, may hold values from 0.1 to 1.9
- pool_scale: float32 [2048], P('tp'), may hold values from 0.1 to 1.9
- w_in: bfloat16 [2048, 2048], P(None, 'tp'), may hold values from -0.125 to 0.125
- w_mix_out: bfloat16 [2048, 2048], P(None, 'tp'), may hold values from -0.125 to 0.125
- expert_gain: float32 [2048], replicated, may hold values from 0.1 to 1.9
- expert_gate: bfloat16 [8, 2048, 2048], P('ep', None, 'tp'), may hold values from -0.125 to 0.125
- expert_up: bfloat16 [8, 2048, 2048], P('ep', None, 'tp'), may hold values from -0.125 to 0.125
- expert_down: bfloat16 [8, 2048, 2048], P('ep', None, 'tp'), may hold values from -0.125 to 0.125
- routes: int32 [4096, 2], P('ep'), may hold values from 0 to 7, all different within a row; in each aligned block of 512 rows (0 to 511, 512 to 1023, ...) at most 192 rows name the same one
- route_weight: float32 [4096, 2], P('ep'), may hold values from 0.1 to 1
Outputs:
- mixer_output: bfloat16 [4096, 2048], P('ep', 'tp')
- expert_output: bfloat16 [4096, 2048], P('ep', 'tp')
Inputs may be any that keep to these rules, and one draw needn't show every extreme that they name: `routes`: each row names 2 different experts. Among the rows of one device (aligned blocks of 512 rows) no expert is named more than 192 times, a bound that some block reaches.
All inputs are finite; a program needn't handle non-finite values.
Results may differ from a plain program's by a relative error of at most 0.0071.
Values may be sent and summed in bfloat16 or wider, within the bound.
A program may use at most 64 MiB of HBM per device.

v0:
```python
import jax
import jax.numpy as jnp
from jax import lax
from jax.sharding import PartitionSpec as P

PW = 2048
TOP = 2


norm_eps = 1e-05
pool_windows = (2, 4, 8, 16)
rim_rows = 8


def extended_2(block, sides, width):
    for axis, dim in sides:
        count = lax.axis_size(axis)
        forward = [(i, i + 1) for i in range(count - 1)]
        backward = [(target, source) for source, target in forward]
        low = lax.ppermute(
            lax.slice_in_dim(block, block.shape[dim] - width, None, axis=dim), axis, forward
        )
        high = lax.ppermute(lax.slice_in_dim(block, 0, width, axis=dim), axis, backward)
        block = jnp.concatenate([low, block, high], axis=dim)
    return block


def layer_norm(row_block, gain_vec):
    values = row_block.astype(jnp.float32)
    center = values - jnp.mean(values, axis=-1, keepdims=True)
    spread = jnp.mean(center * center, axis=-1, keepdims=True)
    return (center * lax.rsqrt(spread + norm_eps) * gain_vec).astype(jnp.bfloat16)


def pooled_channels(inner_t, scale_local, ep_size, ep_index, tp_index):
    extended = extended_2(inner_t, (("ep", 1),), rim_rows).astype(jnp.float32)
    values = inner_t.astype(jnp.float32)
    channels = values.shape[0]
    row_count = values.shape[1]
    seq_len = row_count * ep_size
    position = ep_index * row_count + jnp.arange(row_count, dtype=jnp.int32)
    channel = tp_index * channels + jnp.arange(channels, dtype=jnp.int32)
    group = channel // (PW // 4)
    running = jnp.zeros((channels, row_count), jnp.float32)
    result = jnp.zeros((channels, row_count), jnp.float32)
    last_half = 0
    for group_id, window in enumerate(pool_windows):
        half_span = window // 2
        for offset in list(range(-half_span, -last_half)) + list(range(last_half, half_span)):
            running = running + extended[:, rim_rows + offset : rim_rows + offset + row_count]
        last_half = half_span
        lower_end = jnp.clip(position - half_span, 0, seq_len)
        upper_end = jnp.clip(position - half_span + window, 0, seq_len)
        counts = (upper_end - lower_end).astype(jnp.float32)
        member = (group == group_id)[:, None]
        result = jnp.where(member, running / counts[None, :], result)
    return ((result - values) * scale_local[:, None]).astype(jnp.bfloat16)


def on_device(
    mixer_rows,
    expert_rows,
    mixer_gain,
    pool_scale,
    w_in,
    w_mix_out,
    expert_gain,
    expert_gate,
    expert_up,
    expert_down,
    routes,
    route_weight,
):
    ep_size = lax.axis_size("ep")
    ep_index = lax.axis_index("ep")
    tp_index = lax.axis_index("tp")
    row_count = routes.shape[0]
    capacity = (3 * TOP * row_count + 2 * ep_size - 1) // (2 * ep_size)
    flat_route = routes.reshape(-1)
    onehot = (flat_route[:, None] == jnp.arange(ep_size, dtype=jnp.int32)[None, :]).astype(
        jnp.int32
    )
    ranking = jnp.sum(onehot * (jnp.cumsum(onehot, axis=0) - 1), axis=1)
    target = flat_route * capacity + ranking
    sender = (
        jnp.zeros((ep_size * capacity,), jnp.int32)
        .at[target]
        .set(jnp.arange(row_count * TOP, dtype=jnp.int32) // TOP + 1)
    )
    filled = (sender > 0)[:, None]
    source_row = jnp.maximum(sender - 1, 0)
    full_mix = lax.all_gather(mixer_rows, "tp", axis=1, tiled=True)
    feature_count = expert_rows.shape[1]
    outgoing = jnp.where(filled, expert_rows[source_row], jnp.zeros((), jnp.bfloat16))
    arrived = lax.all_to_all(
        outgoing.reshape(ep_size, capacity, feature_count),
        "ep",
        split_axis=0,
        concat_axis=0,
        tiled=True,
    )
    slot_slices = arrived.reshape(ep_size * capacity, feature_count)
    slot_normed = layer_norm(lax.all_gather(slot_slices, "tp", axis=1, tiled=True), expert_gain)
    contract_first = (((0,), (1,)), ((), ()))
    normed_mix = layer_norm(full_mix, mixer_gain)
    inner_t = lax.dot_general(
        w_in, normed_mix, contract_first, preferred_element_type=jnp.float32
    ).astype(jnp.bfloat16)
    pooled_t = pooled_channels(inner_t, pool_scale, ep_size, ep_index, tp_index)
    gate_t = lax.dot_general(
        expert_gate[0], slot_normed, contract_first, preferred_element_type=jnp.float32
    )
    up_t = lax.dot_general(
        expert_up[0], slot_normed, contract_first, preferred_element_type=jnp.float32
    )
    hidden_t = (jax.nn.silu(gate_t) * up_t).astype(jnp.bfloat16)
    contract_lead = (((0,), (0,)), ((), ()))
    down_weight = expert_down[0]
    mixed_sum = lax.dot_general(
        lax.all_gather(pooled_t, "tp", axis=0, tiled=True),
        w_mix_out,
        contract_lead,
        preferred_element_type=jnp.float32,
    )
    expert_sum = lax.dot_general(
        lax.all_gather(hidden_t, "tp", axis=0, tiled=True),
        down_weight,
        contract_lead,
        preferred_element_type=jnp.float32,
    )
    mixer_output = mixed_sum.astype(jnp.bfloat16)
    back_rows = expert_sum.astype(jnp.bfloat16).reshape(ep_size, capacity, expert_sum.shape[1])
    returned = lax.all_to_all(back_rows, "ep", split_axis=0, concat_axis=0, tiled=True).reshape(
        ep_size * capacity, expert_sum.shape[1]
    )
    picked = returned[target].astype(jnp.float32).reshape(row_count, TOP, expert_sum.shape[1])
    expert_output = jnp.sum(picked * route_weight[:, :, None], axis=1).astype(jnp.bfloat16)
    return (mixer_output, expert_output)


def solution(mesh):
    return jax.shard_map(
        on_device,
        mesh=mesh,
        in_specs=(
            P("ep", "tp"),
            P("ep", "tp"),
            P(),
            P("tp"),
            P(None, "tp"),
            P(None, "tp"),
            P(),
            P("ep", None, "tp"),
            P("ep", None, "tp"),
            P("ep", None, "tp"),
            P("ep", None),
            P("ep", None),
        ),
        out_specs=(P("ep", "tp"), P("ep", "tp")),
        check_vma=False,
    )
```

profile of v0, /device:TPU:0, one launch (start us, length us, event | category | flops | bytes accessed | tf_op | source)
XLA Modules:
  0.0 316.2 jit_solution(4581051959690600166)
XLA Ops:
  7.2 1.0 copy.16
  8.6 0.7 broadcast_multiply_fusion.1
  9.3 2.3 reduce-window.6
  12.5 4.3 %scatter_custom_fusion = s32[1536]{0:T(1024)S(1)} fusion(s32[1024]{0:T(1024)S(1)} %bitcast.50, s32[1024]{0:T(1024)S(1)} %fusion.34, s32[]{:T(128)} %constant.78.clone.1), kind=kCustom, calls=%fused_computation.76 | custom fusion | bytes 6148 | tf_op jit(solution)/shard_map/scatter | solution.py:88
  16.9 5.4 %gather_fusion = bf16[1536,512]{1,0:T(8,128)(2,1)} fusion(bf16[512,512]{1,0:T(8,128)(2,1)S(1)} %copy-done.1, s32[2048]{0:T(1024)S(1)} %pad_clamp_fusion), kind=kCustom, calls=%fused_computation | custom fusion | bytes 3151872 | tf_op jit(solution)/shard_map/gather | solution.py:94
  22.3 1.7 broadcast_select_fusion
  24.0 44.1 %all_to_all.10 = bf16[8,192,512]{2,1,0:T(8,128)(2,1)} all-to-all(bf16[8,192,512]{2,1,0:T(8,128)(2,1)S(1)} %broadcast_select_fusion), channel_id=1, replica_groups=mesh['ep'=8,'tp'=4] {'ep'}, dimensions={0} | all-to-all | bytes 3145728 | tf_op jit(solution)/shard_map/all_to_all | solution.py:95
  68.2 0.7 all-gather.5.cloned.1.call-update
  68.9 68.2 %all-gather.9.cloned.1.call-done = bf16[1536,2048]{1,0:T(8,128)(2,1)} async-done(((bf16[1536,512]{1,0:T(8,128)(2,1)}), bf16[1536,2048]{1,0:T(8,128)(2,1)}) %all-gather.9.cloned.1.call-update) | async-done | bytes 6291472 | tf_op jit(solution)/shard_map/all_gather | solution.py:103
  137.1 3.8 %convert_reduce_fusion = f32[1536]{0:T(1024)S(1)} fusion(bf16[1536,2048]{1,0:T(8,128)(2,1)} %all-gather.9.cloned.1.call-done), kind=kLoop, calls=%fused_computation.4 | loop fusion | flops 6289920 | bytes 6297600 | tf_op jit(solution)/shard_map/reduce_sum | solution.py:30
  140.9 0.8 copy-done.2
  141.7 1.8 fusion.2
  143.5 2.4 fusion.4
  146.0 3.4 %convolution_bitcast_fusion.1 = f32[512,1536]{0,1:T(8,128)S(1)} fusion(bf16[1536,2048]{1,0:T(8,128)(2,1)S(1)} %fusion.4, bf16[1,2048,512]{2,1,0:T(8,128)(2,1)S(1)} %copy-done), kind=kOutput, calls=%fused_computation.19 | convolution fusion | flops 3221225472 | bytes 11534336 | tf_op jit(solution)/shard_map/dot_general | solution.py:110
  149.4 4.8 %fusion.11 = bf16[512,1536]{0,1:T(8,128)(2,1)} fusion(bf16[1536,2048]{1,0:T(8,128)(2,1)S(1)} %fusion.4, f32[512,1536]{0,1:T(8,128)S(1)} %convolution_bitcast_fusion.1, bf16[1,2048,512]{2,1,0:T(8,128)(2,1)S(1)} %copy-done.7), kind=kOutput, calls=%fused_computation.20 | convolution fusion | flops 3225944064 | bytes 13107200 | tf_op jit(solution)/shard_map/dot_general | solution.py:113
  154.5 19.4 %all-gather.5.cloned.1.call-done = bf16[512,2048]{1,0:T(8,128)(2,1)} async-done(((bf16[512,512]{1,0:T(8,128)(2,1)}), bf16[512,2048]{1,0:T(8,128)(2,1)}) %all-gather.5.cloned.1.call-update) | async-done | bytes 2097168 | tf_op jit(solution)/shard_map/all_gather | solution.py:92
  174.0 2.1 convert_reduce_fusion.1
  176.2 0.7 fusion.7
  176.9 1.3 fusion.23
  178.3 1.6 collective-permute-start
  179.9 1.3 collective-permute-start.1
  181.2 3.2 %collective-permute-done.1 = bf16[512,8]{0,1:T(8,128)(2,1)S(1)} collective-permute-done((bf16[512,8]{0,1:T(8,128)(2,1)S(1)}, bf16[512,8]{0,1:T(8,128)(2,1)S(1)}, u32[]{:S(2)}, u32[]{:S(2)}) %collective-permute-start.1) | collective-permute-done | bytes 8224 | tf_op jit(solution)/shard_map/ppermute | solution.py:23
  184.5 3.3 %fusion.30 = bf16[512,512]{0,1:T(8,128)(2,1)} fusion(bf16[512,512]{0,1:T(8,128)(2,1)S(1)} %fusion.23, f32[512,528]{0,1:T(8,128)S(1)} %maximum_convert_fusion, f32[512]{0:T(512)S(1)} %copy-done.6, f32[512]{0:T(512)S(1)} %get-tuple-element.4, f32[512]{0:T(512)S(1)} %get-tuple-element.5, f32[512]{0:T(512)S(1)} %get-tuple-element.6, ...), kind=kLoop, calls=%fused_computation.53 | loop fusion | flops 7077888 | bytes 17838080 | tf_op jit(solution)/shard_map/convert_element_type | solution.py:57
  187.8 57.9 %all-gather.11.cloned.1.call-done = bf16[2048,1536]{0,1:T(8,128)(2,1)} async-done(((bf16[512,1536]{0,1:T(8,128)(2,1)}), bf16[2048,1536]{0,1:T(8,128)(2,1)}) %all-gather.11.cloned.1.call-update) | async-done | bytes 6291472 | tf_op jit(solution)/shard_map/all_gather | solution.py:126
  245.8 8.1 %convolution_convert_fusion = bf16[1536,512]{1,0:T(8,128)(2,1)} fusion(bf16[2048,1536]{0,1:T(8,128)(2,1)} %all-gather.11.cloned.1.call-done, bf16[1,2048,512]{2,1,0:T(8,128)(2,1)} %param.21), kind=kOutput, calls=%fused_computation.21 | convolution fusion | flops 3222011904 | bytes 9961472 | tf_op jit(solution)/shard_map/dot_general | solution.py:125
  253.8 4.7 %all-to-all-start.1 = ((bf16[8,192,512]{2,1,0:T(8,128)(2,1)}), bf16[8,192,512]{2,1,0:T(8,128)(2,1)}, u32[]{:S(2)}, u32[]{:S(2)}) async-start(bf16[8,192,512]{2,1,0:T(8,128)(2,1)} %bitcast.48), calls=%async_computation.1 | async-start | bytes 3145728 | tf_op jit(solution)/shard_map/all_to_all | solution.py:133
  258.7 24.3 %all-gather.7.cloned.1.call-done = bf16[2048,512]{0,1:T(8,128)(2,1)} async-done(((bf16[512,512]{0,1:T(8,128)(2,1)}), bf16[2048,512]{0,1:T(8,128)(2,1)}) %all-gather.7.cloned.1.call-update) | async-done | bytes 2097168 | tf_op jit(solution)/shard_map/all_gather | solution.py:120
  283.1 4.3 %convolution_convert_fusion.1 = bf16[512,512]{1,0:T(8,128)(2,1)} fusion(bf16[2048,512]{0,1:T(8,128)(2,1)} %all-gather.7.cloned.1.call-done, bf16[2048,512]{1,0:T(8,128)(2,1)} %param.17), kind=kOutput, calls=%fused_computation.32 | convolution fusion | flops 1074003968 | bytes 4718592 | tf_op jit(solution)/shard_map/dot_general | solution.py:119
  287.4 9.1 %all-to-all-done.1 = bf16[8,192,512]{2,1,0:T(8,128)(2,1)} async-done(((bf16[8,192,512]{2,1,0:T(8,128)(2,1)}), bf16[8,192,512]{2,1,0:T(8,128)(2,1)}, u32[]{:S(2)}, u32[]{:S(2)}) %all-to-all-start.1) | async-done | bytes 1572896 | tf_op jit(solution)/shard_map/all_to_all | solution.py:133
  296.5 5.6 %gather_fusion.1 = bf16[1024,512]{1,0:T(8,128)(2,1)S(1)} fusion(bf16[1536,512]{1,0:T(8,128)(2,1)} %bitcast.12, s32[1024]{0:T(1024)S(1)} %broadcast_clamp_fusion), kind=kCustom, calls=%fused_computation.1 | custom fusion | bytes 2101248 | tf_op jit(solution)/shard_map/gather | solution.py:136
  302.1 2.4 reshape.168
  304.4 5.2 %multiply_reduce_fusion = bf16[512,512]{1,0:T(8,128)(2,1)} fusion(f32[512,2,512]{2,1,0:T(2,128)} %reshape.168, f32[512,2]{1,0:T(8,128)S(1)} %copy.18), kind=kLoop, calls=%fused_computation.26 | loop fusion | flops 786432 | bytes 2625536 | tf_op jit(solution)/shard_map/reduce_sum | solution.py:137
  (54 shorter events, 2.2 us)
Async XLA Ops:
  7.2 138.8 %copy-start = (bf16[1,2048,512]{2,1,0:T(8,128)(2,1)S(1)}, bf16[1,2048,512]{2,1,0:T(8,128)(2,1)}, u32[]{:S(2)}) copy-start(bf16[1,2048,512]{2,1,0:T(8,128)(2,1)} %param.19) | copy-start | bytes 6291460
  7.2 9.8 %copy-start.1 = (bf16[512,512]{1,0:T(8,128)(2,1)S(1)}, bf16[512,512]{1,0:T(8,128)(2,1)}, u32[]{:S(2)}) copy-start(bf16[512,512]{1,0:T(8,128)(2,1)} %param.13) | copy-start | bytes 1572868
  7.2 129.9 %all-gather.9.cloned.1.call-start = ((), (), s32[]{:S(2)}) async-start(), calls=%async_computation.4 | async-start | bytes 7864320 | tf_op jit(solution)/shard_map/all_gather | solution.py:103
  68.1 105.9 %all-gather.5.cloned.1.call-start = ((), (), s32[]{:S(2)}) async-start(), calls=%async_computation.2 | async-start | bytes 2621440 | tf_op jit(solution)/shard_map/all_gather | solution.py:92
  68.9 176.9 %all-gather.11.cloned.1.call-start = ((), (), s32[]{:S(2)}) async-start(), calls=%async_computation.5 | async-start | bytes 7864320 | tf_op jit(solution)/shard_map/all_gather | solution.py:126
  137.1 4.6 %copy-start.2 = (bf16[1536,2048]{1,0:T(8,128)(2,1)S(1)}, bf16[1536,2048]{1,0:T(8,128)(2,1)}, u32[]{:S(2)}) copy-start(bf16[1536,2048]{1,0:T(8,128)(2,1)} %all-gather.9.cloned.1.call-done) | copy-start | bytes 18874372
  141.7 1.8 copy-start.4
  145.9 3.5 %copy-start.7 = (bf16[1,2048,512]{2,1,0:T(8,128)(2,1)S(1)}, bf16[1,2048,512]{2,1,0:T(8,128)(2,1)}, u32[]{:S(2)}) copy-start(bf16[1,2048,512]{2,1,0:T(8,128)(2,1)} %param.20) | copy-start | bytes 6291460
  154.3 128.8 %all-gather.7.cloned.1.call-start = ((), (), s32[]{:S(2)}) async-start(), calls=%async_computation.3 | async-start | bytes 2621440 | tf_op jit(solution)/shard_map/all_gather | solution.py:120
  174.0 2.2 copy-start.3
  174.0 2.9 copy-start.8
  174.0 2.9 copy-start.9
  176.9 7.6 %copy-start.6 = (f32[512]{0:T(512)S(1)}, f32[512]{0:T(512)}, u32[]{:S(2)}) copy-start(f32[512]{0:T(512)} %param.15) | copy-start | bytes 6148
  178.3 2.9 collective-permute-start
  179.9 4.5 %collective-permute-start.1 = (bf16[512,8]{0,1:T(8,128)(2,1)S(1)}, bf16[512,8]{0,1:T(8,128)(2,1)S(1)}, u32[]{:S(2)}, u32[]{:S(2)}) collective-permute-start(bf16[512,8]{0,1:T(8,128)(2,1)S(1)} %get-tuple-element.3), channel_id=1, source_target_pairs={{4,0},{8,4},{12,8},{16,12},{20,16},{24,20},{28,24},{5,1},{9,5},{13... | collective-permute-start | bytes 24584 | tf_op jit(solution)/shard_map/ppermute | solution.py:23
  253.8 4.7 %copy-start.5 = (f32[512,2]{0,1:T(2,128)S(1)}, f32[512,2]{0,1:T(2,128)}, u32[]{:S(2)}) copy-start(f32[512,2]{0,1:T(2,128)} %param.23) | copy-start | bytes 12292
  253.8 42.6 %all-to-all-start.1 = ((bf16[8,192,512]{2,1,0:T(8,128)(2,1)}), bf16[8,192,512]{2,1,0:T(8,128)(2,1)}, u32[]{:S(2)}, u32[]{:S(2)}) async-start(bf16[8,192,512]{2,1,0:T(8,128)(2,1)} %bitcast.48), calls=%async_computation.1 | async-start | bytes 3145728 | tf_op jit(solution)/shard_map/all_to_all | solution.py:133
Sparse Core Ops, SparseCore 0:
  68.2 68.8 all-gather.8
  138.9 35.0 all-gather.4
  175.8 69.8 all-gather.10
  248.0 35.0 all-gather.6
where the time goes:
time: 317 us; the launch traced here: 316 us
  waiting for transfers between devices  183 us (58%)
  blocking collectives  44.1 us (14%)
  other arithmetic  24.5 us (8%)
  matrix products  21.9 us (7%)
  local copies, waits for them, and re-layouts  20.8 us (7%)
  between operations  14.1 us (4%)
  starting transfers between devices  7.95 us (3%)
    all_gather x1, waiting for transfers between devices, on_device(): lax.all_gather(slot_slices, 'tp', axis=1, tiled=True)  68.2 us
    all_gather x1, waiting for transfers between devices, on_device(): lax.all_gather(hidden_t, 'tp', axis=0, tiled=True)  57.9 us
    all_to_all x1, blocking collectives, on_device(): lax.all_to_all(outgoing.reshape(ep_size, capacity, feature_count), 'ep',...  44.1 us
    all_gather x1, waiting for transfers between devices, on_device(): lax.all_gather(pooled_t, 'tp', axis=0, tiled=True)  24.3 us
    all_gather x1, waiting for transfers between devices, on_device(): full_mix = lax.all_gather(mixer_rows, 'tp', axis=1, tiled=True)  19.4 us
    all_to_all x1, waiting for transfers between devices, on_device(): lax.all_to_all(back_rows, 'ep', split_axis=0, concat_axis=0, tiled=True)  9.13 us
    dot_general x1, matrix products, on_device(): lax.dot_general(lax.all_gather(hidden_t, 'tp', axis=0, tiled=True), down_...  8.08 us
  transfers between devices with their start and end apart: 7, of which 6 were waited for; matrix products, arithmetic and copies ran while one was open for 12% of the time, Pallas kernels for 0%

commit v1 on v0

v1 whole, which is shorter than its diff:
```python
import functools

import jax
import jax.numpy as jnp
from jax import lax
from jax.experimental import pallas as pl
from jax.experimental.pallas import tpu as pltpu
from jax.sharding import PartitionSpec as P

TOP = 2
norm_eps = 1e-05
pool_windows = (2, 4, 8, 16)
RIM = 16
MESH = pl.DeviceIdType.MESH
f32 = jnp.float32
bf16 = jnp.bfloat16


def fused(
    ep,
    tp,
    xm_in,
    xe_in,
    gain_m,
    gain_e,
    scale,
    trow,
    tcol,
    rw,
    w_in_h,
    w_mix_h,
    gate_h,
    up_h,
    down_h,
    out_m,
    out_e,
    w_in,
    w_mix,
    gate,
    up,
    down,
    xm,
    xe,
    normed,
    disp_send,
    disp_recv,
    hid,
    pooled,
    back_send,
    back_recv,
    ext,
    rim_send,
    rim_recv,
    acc,
    w_sem,
    xe_s,
    xe_r,
    xm_s,
    xm_r,
    dp_s,
    dp_r,
    rim_s,
    rim_r,
    po_s,
    po_r,
    hi_s,
    hi_r,
    bk_s,
    bk_r,
):
    me_ep = lax.axis_index("ep")
    me_tp = lax.axis_index("tp")
    rows, feat = xm_in.shape
    cap = disp_recv.shape[1]
    chan = out_m.shape[1]
    width = feat * tp
    chunk = min(rows, 128)

    barrier = pltpu.get_barrier_semaphore()
    for d in range(1, tp):
        pl.semaphore_signal(
            barrier, inc=1, device_id={"tp": lax.rem(me_tp + d, tp)}, device_id_type=MESH
        )
    for d in range(1, ep):
        pl.semaphore_signal(
            barrier, inc=1, device_id={"ep": lax.rem(me_ep + d, ep)}, device_id_type=MESH
        )
    pl.semaphore_wait(barrier, tp + ep - 2)

    def tp_copy(src, dst, s, r, d):
        return pltpu.make_async_remote_copy(
            src_ref=src,
            dst_ref=dst,
            send_sem=s,
            recv_sem=r,
            device_id={"tp": lax.rem(me_tp + d, tp)},
            device_id_type=MESH,
        )

    def ep_copy(src, dst, s, r, d):
        return pltpu.make_async_remote_copy(
            src_ref=src,
            dst_ref=dst,
            send_sem=s,
            recv_sem=r,
            device_id={"ep": lax.rem(me_ep + d, ep)},
            device_id_type=MESH,
        )

    def tp_from(d):
        return lax.rem(me_tp - d + tp, tp)

    def ep_from(d):
        return lax.rem(me_ep - d + ep, ep)

    for d in range(1, tp):
        tp_copy(xe_in, xe.at[me_tp], xe_s.at[d - 1], xe_r.at[d - 1], d).start()
    for d in range(1, tp):
        tp_copy(xm_in, xm.at[me_tp], xm_s.at[d - 1], xm_r.at[d - 1], d).start()

    loads = [
        pltpu.make_async_copy(h, v, w_sem.at[i])
        for i, (h, v) in enumerate(
            ((w_in_h, w_in), (gate_h, gate), (up_h, up), (w_mix_h, w_mix), (down_h, down))
        )
    ]
    for load in loads:
        load.start()

    xe[me_tp] = xe_in[...]
    xm[me_tp] = xm_in[...]

    def norm_into(gathered, gain):
        def step(i, carry):
            at = pl.ds(pl.multiple_of(i * chunk, chunk), chunk)
            parts = [gathered[p, at, :].astype(f32) for p in range(tp)]
            total = sum(jnp.sum(v, axis=-1, keepdims=True) for v in parts)
            mean = total / width
            parts = [v - mean for v in parts]
            spread = sum(jnp.sum(v * v, axis=-1, keepdims=True) for v in parts) / width
            inv = lax.rsqrt(spread + norm_eps)
            for p in range(tp):
                cols = slice(p * feat, (p + 1) * feat)
                normed[at, cols] = (parts[p] * inv * gain[:, cols]).astype(bf16)
            return carry

        lax.fori_loop(0, rows // chunk, step, 0)

    for d in range(1, tp):
        tp_copy(xe_in, xe.at[tp_from(d)], xe_s.at[d - 1], xe_r.at[d - 1], d).wait_recv()
    norm_into(xe, gain_e)

    def picked_rows(e):
        slot = lax.broadcasted_iota(jnp.int32, (cap, rows), 0) + e * cap
        hit = (slot == trow[0:1, :]) | (slot == trow[1:2, :])
        pick = jnp.where(hit, 1.0, 0.0).astype(bf16)
        return jnp.dot(pick, normed[...], preferred_element_type=f32).astype(bf16)

    def send_rows(d, carry):
        e = lax.rem(me_ep + d, ep)
        disp_send[e] = picked_rows(e)
        ep_copy(disp_send.at[e], disp_recv.at[me_ep], dp_s.at[d], dp_r.at[d], d).start()
        return carry

    lax.fori_loop(1, ep, send_rows, 0)
    disp_recv[me_ep] = picked_rows(me_ep)

    for d in range(1, tp):
        tp_copy(xm_in, xm.at[tp_from(d)], xm_s.at[d - 1], xm_r.at[d - 1], d).wait_recv()
    norm_into(xm, gain_m)
    loads[0].wait()

    def project(i, carry):
        at = pl.ds(pl.multiple_of(i * chunk, chunk), chunk)
        inner = jnp.dot(normed[at, :], w_in[...], preferred_element_type=f32).astype(bf16)
        ext[pl.ds(pl.multiple_of(RIM + i * chunk, RIM), chunk), :] = inner.astype(f32)
        return carry

    lax.fori_loop(0, rows // chunk, project, 0)
    rim_send[0] = ext[rows : rows + RIM, :].astype(bf16)
    rim_send[1] = ext[RIM : 2 * RIM, :].astype(bf16)
    up_rim = ep_copy(rim_send.at[0], rim_recv.at[0], rim_s.at[0], rim_r.at[0], 1)
    down_rim = ep_copy(rim_send.at[1], rim_recv.at[1], rim_s.at[1], rim_r.at[1], ep - 1)
    up_rim.start()
    down_rim.start()

    loads[1].wait()
    loads[2].wait()

    def hidden_of(q):
        x = disp_recv[q]
        g = jnp.dot(x, gate[...], preferred_element_type=f32)
        u = jnp.dot(x, up[...], preferred_element_type=f32)
        return (g / (1.0 + jnp.exp(-g)) * u).astype(bf16)

    hid[me_ep, me_tp] = hidden_of(me_ep)

    up_rim.wait_recv()
    down_rim.wait_recv()
    low = rim_recv[0].astype(f32)
    high = rim_recv[1].astype(f32)
    ext[0:RIM, :] = jnp.where(me_ep > 0, low, 0.0)
    ext[RIM + rows : 2 * RIM + rows, :] = jnp.where(me_ep < ep - 1, high, 0.0)

    group_width = chan * tp // len(pool_windows)
    channel = me_tp * chan + lax.broadcasted_iota(jnp.int32, (1, chan), 1)
    seq_len = rows * ep
    for i in range(rows // chunk):
        first = RIM + i * chunk
        position = me_ep * rows + i * chunk + lax.broadcasted_iota(jnp.int32, (chunk, 1), 0)
        running = jnp.zeros((chunk, chan), f32)
        result = jnp.zeros((chunk, chan), f32)
        last = 0
        for g, window in enumerate(pool_windows):
            half = window // 2
            for o in list(range(-half, -last)) + list(range(last, half)):
                running = running + ext[first + o : first + o + chunk, :]
            last = half
            lower = jnp.maximum(position - half, 0)
            upper = jnp.minimum(position + half, seq_len)
            counts = (upper - lower).astype(f32)
            member = (channel >= g * group_width) & (channel < (g + 1) * group_width)
            result = jnp.where(member, running / counts, result)
        values = ext[first : first + chunk, :]
        pooled[me_tp, i * chunk : (i + 1) * chunk, :] = (
            (result - values) * scale[...]
        ).astype(bf16)
    for d in range(1, tp):
        tp_copy(pooled.at[me_tp], pooled.at[me_tp], po_s.at[d - 1], po_r.at[d - 1], d).start()

    def send_hidden(q, k):
        for d in range(1, tp):
            tp_copy(
                hid.at[q, me_tp], hid.at[q, me_tp], hi_s.at[k, d - 1], hi_r.at[k, d - 1], d
            ).start()

    send_hidden(me_ep, 0)

    def expert(k, carry):
        q = ep_from(k)
        ep_copy(disp_send.at[q], disp_recv.at[q], dp_s.at[k], dp_r.at[k], k).wait_recv()
        hid[q, me_tp] = hidden_of(q)
        send_hidden(q, k)
        return carry

    lax.fori_loop(1, ep, expert, 0)

    loads[3].wait()
    for d in range(1, tp):
        tp_copy(
            pooled.at[me_tp], pooled.at[tp_from(d)], po_s.at[d - 1], po_r.at[d - 1], d
        ).wait_recv()

    def mix_out(i, carry):
        at = pl.ds(pl.multiple_of(i * chunk, chunk), chunk)
        total = jnp.zeros((chunk, chan), f32)
        for p in range(tp):
            total = total + jnp.dot(
                pooled[p, at, :],
                w_mix[p * chan : (p + 1) * chan, :],
                preferred_element_type=f32,
            )
        out_m[at, :] = total.astype(bf16)
        return carry

    lax.fori_loop(0, rows // chunk, mix_out, 0)
    loads[4].wait()
    units = hid.shape[3]

    def value_of(q, k):
        for d in range(1, tp):
            tp_copy(
                hid.at[q, me_tp], hid.at[q, tp_from(d)], hi_s.at[k, d - 1], hi_r.at[k, d - 1], d
            ).wait_recv()
        total = jnp.zeros((cap, out_e.shape[1]), f32)
        for p in range(tp):
            total = total + jnp.dot(
                hid[q, p],
                down[p * units : (p + 1) * units, :],
                preferred_element_type=f32,
            )
        return total.astype(bf16)

    back_recv[me_ep] = value_of(me_ep, 0)

    def send_value(k, carry):
        q = ep_from(k)
        back_send[q] = value_of(q, k)
        ep_copy(
            back_send.at[q], back_recv.at[me_ep], bk_s.at[k], bk_r.at[k], ep - k
        ).start()
        return carry

    lax.fori_loop(1, ep, send_value, 0)

    def combine(e):
        slot = lax.broadcasted_iota(jnp.int32, (rows, cap), 1) + e * cap
        weight = jnp.where(slot == tcol[:, 0:1], rw[:, 0:1], 0.0) + jnp.where(
            slot == tcol[:, 1:2], rw[:, 1:2], 0.0
        )
        coarse = weight.astype(bf16)
        fine = (weight - coarse.astype(f32)).astype(bf16)
        v = back_recv[e]
        return jnp.dot(coarse, v, preferred_element_type=f32) + jnp.dot(
            fine, v, preferred_element_type=f32
        )

    acc[...] = combine(me_ep)

    def gather_value(k, carry):
        e = lax.rem(me_ep + k, ep)
        ep_copy(back_send.at[e], back_recv.at[e], bk_s.at[k], bk_r.at[k], k).wait_recv()
        acc[...] += combine(e)
        return carry

    lax.fori_loop(1, ep, gather_value, 0)
    out_e[...] = acc[...].astype(bf16)

    for d in range(1, tp):
        tp_copy(xe_in, xe.at[me_tp], xe_s.at[d - 1], xe_r.at[d - 1], d).wait_send()
        tp_copy(xm_in, xm.at[me_tp], xm_s.at[d - 1], xm_r.at[d - 1], d).wait_send()
        tp_copy(
            pooled.at[me_tp], pooled.at[me_tp], po_s.at[d - 1], po_r.at[d - 1], d
        ).wait_send()
    up_rim.wait_send()
    down_rim.wait_send()

    def drain(k, carry):
        e = lax.rem(me_ep + k, ep)
        q = ep_from(k)
        ep_copy(disp_send.at[e], disp_recv.at[me_ep], dp_s.at[k], dp_r.at[k], k).wait_send()
        ep_copy(back_send.at[q], back_recv.at[me_ep], bk_s.at[k], bk_r.at[k], ep - k).wait_send()
        return carry

    lax.fori_loop(1, ep, drain, 0)

    def drain_hidden(k, carry):
        q = ep_from(k)
        for d in range(1, tp):
            tp_copy(
                hid.at[q, me_tp], hid.at[q, me_tp], hi_s.at[k, d - 1], hi_r.at[k, d - 1], d
            ).wait_send()
        return carry

    lax.fori_loop(0, ep, drain_hidden, 0)


def on_device(
    mixer_rows,
    expert_rows,
    mixer_gain,
    pool_scale,
    w_in,
    w_mix_out,
    expert_gain,
    expert_gate,
    expert_up,
    expert_down,
    routes,
    route_weight,
    *,
    ep,
    tp,
):
    rows, feat = mixer_rows.shape
    width = feat * tp
    cap = (3 * TOP * rows + 2 * ep - 1) // (2 * ep)
    chan = w_in.shape[1]
    units = expert_gate.shape[2]
    flat_route = routes.reshape(-1)
    onehot = (flat_route[:, None] == jnp.arange(ep, dtype=jnp.int32)[None, :]).astype(jnp.int32)
    ranking = jnp.sum(onehot * (jnp.cumsum(onehot, axis=0) - 1), axis=1)
    target = (flat_route * cap + ranking).reshape(rows, TOP)

    vmem = pl.BlockSpec(memory_space=pltpu.VMEM)
    hbm = pl.BlockSpec(memory_space=pl.ANY)
    dma = pltpu.SemaphoreType.DMA
    return pl.pallas_call(
        functools.partial(fused, ep, tp),
        out_shape=(
            jax.ShapeDtypeStruct((rows, w_mix_out.shape[1]), bf16),
            jax.ShapeDtypeStruct((rows, expert_down.shape[2]), bf16),
        ),
        in_specs=[vmem] * 8 + [hbm] * 5,
        out_specs=(vmem, vmem),
        scratch_shapes=[
            pltpu.VMEM(w_in.shape, bf16),
            pltpu.VMEM(w_mix_out.shape, bf16),
            pltpu.VMEM(expert_gate.shape[1:], bf16),
            pltpu.VMEM(expert_up.shape[1:], bf16),
            pltpu.VMEM(expert_down.shape[1:], bf16),
            pltpu.VMEM((tp, rows, feat), bf16),
            pltpu.VMEM((tp, rows, feat), bf16),
            pltpu.VMEM((rows, width), bf16),
            pltpu.VMEM((ep, cap, width), bf16),
            pltpu.VMEM((ep, cap, width), bf16),
            pltpu.VMEM((ep, tp, cap, units), bf16),
            pltpu.VMEM((tp, rows, chan), bf16),
            pltpu.VMEM((ep, cap, expert_down.shape[2]), bf16),
            pltpu.VMEM((ep, cap, expert_down.shape[2]), bf16),
            pltpu.VMEM((rows + 2 * RIM, chan), f32),
            pltpu.VMEM((2, RIM, chan), bf16),
            pltpu.VMEM((2, RIM, chan), bf16),
            pltpu.VMEM((rows, expert_down.shape[2]), f32),
            dma((5,)),
            dma((tp - 1,)),
            dma((tp - 1,)),
            dma((tp - 1,)),
            dma((tp - 1,)),
            dma((ep,)),
            dma((ep,)),
            dma((2,)),
            dma((2,)),
            dma((tp - 1,)),
            dma((tp - 1,)),
            dma((ep, tp - 1)),
            dma((ep, tp - 1)),
            dma((ep,)),
            dma((ep,)),
        ],
        compiler_params=pltpu.CompilerParams(
            collective_id=0, has_side_effects=True, vmem_limit_bytes=62 * 1024 * 1024
        ),
    )(
        mixer_rows,
        expert_rows,
        mixer_gain.reshape(1, width),
        expert_gain.reshape(1, width),
        pool_scale.reshape(1, chan),
        target.T,
        target,
        route_weight,
        w_in,
        w_mix_out,
        expert_gate.reshape(expert_gate.shape[1:]),
        expert_up.reshape(expert_up.shape[1:]),
        expert_down.reshape(expert_down.shape[1:]),
    )


def solution(mesh):
    return jax.shard_map(
        functools.partial(on_device, ep=mesh.shape["ep"], tp=mesh.shape["tp"]),
        mesh=mesh,
        in_specs=(
            P("ep", "tp"),
            P("ep", "tp"),
            P(),
            P("tp"),
            P(None, "tp"),
            P(None, "tp"),
            P(),
            P("ep", None, "tp"),
            P("ep", None, "tp"),
            P("ep", None, "tp"),
            P("ep", None),
            P("ep", None),
        ),
        out_specs=(P("ep", "tp"), P("ep", "tp")),
        check_vma=False,
    )
```

time: 317 us -> 251 us (0.79)
  Pallas kernels: 0 us -> 238 us
  waiting for transfers between devices: 183 us -> 0 us
  blocking collectives: 44.1 us -> 0 us
  matrix products: 21.9 us -> 0 us
  other arithmetic: 24.5 us -> 3.26 us
  local copies, waits for them, and re-layouts: 20.8 us -> 7.1 us
  between operations: 14.1 us -> 0.71 us
  starting transfers between devices: 7.95 us -> 0 us
    pallas_call x0 -> x1, Pallas kernels: none -> 238 us  [on_device(): pl.pallas_call(functools.partial(fused, ep, tp), out_shape=(jax.ShapeDtyp...]
    all_gather x4 -> x0, waiting for transfers between devices: 170 us -> none  [the longest x1 68.2 us: on_device(): lax.all_gather(slot_slices, 'tp', axis=1, tiled=True)]
    all_to_all x1 -> x0, blocking collectives: 44.1 us -> none  [on_device(): lax.all_to_all(outgoing.reshape(ep_size, capacity, feature_count), 'ep',...]
    dot_general x5 -> x0, matrix products: 21.9 us -> none  [the longest x1 8.08 us: on_device(): lax.dot_general(lax.all_gather(hidden_t, 'tp', axis=0, tiled=True), down_...]
    reduce_sum x5 -> x0, other arithmetic: 13.6 us -> none  [the longest x2 5.91 us: layer_norm(): center = values - jnp.mean(values, axis=-1, keepdims=True)]
    gather x2 -> x0, local copies, waits for them, and re-layouts: 11 us -> none  [the longest x1 5.6 us: on_device(): returned[target].astype(jnp.float32)]
    all_to_all x1 -> x0, waiting for transfers between devices: 9.13 us -> none  [on_device(): lax.all_to_all(back_rows, 'ep', split_axis=0, concat_axis=0, tiled=True)]
    convert_element_type x6 -> x1, other arithmetic: 5.88 us -> 0.01 us  [on_device(): (flat_route[:, None] == jnp.arange(ep, dtype=jnp.int32)[None, :]).astype(...]
  transfers between devices with their start and end apart: 7 -> 0, of which waited for: 6 -> 0; matrix products, arithmetic and copies ran while one was open for 12% -> 0% of each run, Pallas kernels for 0% -> 0%
where the time goes in v1:
time: 251 us; the launch traced here: 249 us
  Pallas kernels  238 us (95%)
  local copies, waits for them, and re-layouts  7.1 us (3%)
  other arithmetic  3.26 us (1%)
    pallas_call x1, Pallas kernels, on_device(): pl.pallas_call(functools.partial(fused, ep, tp), out_shape=(jax.ShapeDtyp...  238 us
    unnamed x8, local copies, waits for them, and re-layouts  5.44 us

profile of v1, /device:TPU:0, one launch (start us, length us, event | category | flops | bytes accessed | tf_op | source)
XLA Modules:
  0.0 249.3 jit_solution(15681699847180778703)
XLA Ops:
  0.6 0.0 copy-start.1
  0.6 0.7 broadcast_multiply_fusion
  1.3 0.1 copy.26
  1.5 0.8 copy.24
  2.3 0.2 eq.29
  2.5 0.2 eq.25
  2.7 2.3 reduce-window.6
  5.0 0.3 slice_reduce_fusion
  5.2 0.2 reduce-window.9
  5.4 0.1 add_bitcast_fusion
  5.5 0.2 reduce_sum.12
  5.7 0.0 copy-start
  5.8 0.7 copy.27.trow
  6.5 0.0 copy-done.1
  6.5 0.9 copy.28.rw
  7.3 0.0 copy-done
  7.3 238.2 %shard_map.131 = (bf16[512,512]{1,0:T(8,128)(2,1)}, bf16[512,512]{1,0:T(8,128)(2,1)}) custom-call(bf16[512,512]{1,0:T(8,128)(2,1)} %xm_in.1, bf16[512,512]{1,0:T(8,128)(2,1)} %xe_in.1, f32[1,2048]{1,0:T(1,128)} %bitcast.27, f32[1,2048]{1,0:T(1,128)} %bitcast.28, f32[1,512]{1,0:T(1,128)} %bitcast.29, s32[2,512]{1,0:T(2,128)} %copy.27.trow, s32[512,2]{1,0:T(8,128)} %copy-done, ...), custom_call_target="tpu_custom_call" | custom-call | tf_op jit(solution)/shard_map/pallas_call | solution.py:378
  245.6 1.9 copy.33
  247.4 1.9 copy.34
  (3 shorter events, 0.1 us)
Async XLA Ops:
  0.6 5.8 %copy-start.1 = (f32[512,2]{0,1:T(2,128)S(1)}, f32[512,2]{0,1:T(2,128)}, u32[]{:S(2)}) copy-start(f32[512,2]{0,1:T(2,128)} %param.23) | copy-start | bytes 12292
  5.7 1.6 copy-start

commit v2 on v1

--- a/solution.py
+++ b/solution.py
@@ -40,10 +40,10 @@
     up,
     down,
     xm,
-    xe,
     normed,
+    block,
     disp_send,
-    disp_recv,
+    slots,
     hid,
     pooled,
     back_send,
@@ -53,8 +53,8 @@
     rim_recv,
     acc,
     w_sem,
-    xe_s,
-    xe_r,
+    sl_s,
+    sl_r,
     xm_s,
     xm_r,
     dp_s,
@@ -71,7 +71,7 @@
     me_ep = lax.axis_index("ep")
     me_tp = lax.axis_index("tp")
     rows, feat = xm_in.shape
-    cap = disp_recv.shape[1]
+    cap = slots.shape[2]
     chan = out_m.shape[1]
     width = feat * tp
     chunk = min(rows, 128)
@@ -87,13 +87,13 @@
         )
     pl.semaphore_wait(barrier, tp + ep - 2)
 
-    def tp_copy(src, dst, s, r, d):
+    def tp_copy(ref, s, r, peer):
         return pltpu.make_async_remote_copy(
-            src_ref=src,
-            dst_ref=dst,
+            src_ref=ref,
+            dst_ref=ref,
             send_sem=s,
             recv_sem=r,
-            device_id={"tp": lax.rem(me_tp + d, tp)},
+            device_id={"tp": peer},
             device_id_type=MESH,
         )
 
@@ -107,16 +107,62 @@
             device_id_type=MESH,
         )
 
-    def tp_from(d):
-        return lax.rem(me_tp - d + tp, tp)
+    relayed = tp == 4
+    col = lax.rem(me_tp, 2)
+    row = me_tp // 2
+    beside = row * 2 + (1 - col)
+    above = (1 - row) * 2 + col
+    across = (1 - row) * 2 + (1 - col)
+
+    def send(slot, s, r):
+        if relayed:
+            tp_copy(slot(me_tp), s(0), r(0), beside).start()
+            tp_copy(slot(me_tp), s(1), r(1), above).start()
+        else:
+            for d in range(1, tp):
+                tp_copy(slot(me_tp), s(d - 1), r(d - 1), lax.rem(me_tp + d, tp)).start()
+
+    def relay(slot, s, r, turn):
+        if relayed:
+            tp_copy(slot(beside), s(0), r(0), beside).wait_recv()
+            tp_copy(slot(above), s(1), r(1), above).wait_recv()
+            source = (1 - turn) * beside + turn * above
+            peer = (1 - turn) * above + turn * beside
+            tp_copy(slot(source), s(2), r(2), peer).start()
+
+    def finish(slot, s, r):
+        if relayed:
+            tp_copy(slot(across), s(2), r(2), across).wait_recv()
+        else:
+            for d in range(1, tp):
+                p = lax.rem(me_tp - d + tp, tp)
+                tp_copy(slot(p), s(d - 1), r(d - 1), p).wait_recv()
+
+    def drain(slot, s, r):
+        for d in range(1, tp):
+            tp_copy(slot(me_tp), s(d - 1), r(d - 1), lax.rem(me_tp + d, tp)).wait_send()
+
+    def mixer_part():
+        return lambda p: xm.at[p], lambda j: xm_s.at[j], lambda j: xm_r.at[j]
+
+    def pooled_part():
+        return lambda p: pooled.at[p], lambda j: po_s.at[j], lambda j: po_r.at[j]
+
+    def slot_part(k):
+        q = ep_from(k)
+        return lambda p: slots.at[q, p], lambda j: sl_s.at[k, j], lambda j: sl_r.at[k, j]
+
+    def hidden_part(k):
+        q = ep_from(k)
+        return lambda p: hid.at[q, p], lambda j: hi_s.at[k, j], lambda j: hi_r.at[k, j]
 
     def ep_from(d):
         return lax.rem(me_ep - d + ep, ep)
 
-    for d in range(1, tp):
-        tp_copy(xe_in, xe.at[me_tp], xe_s.at[d - 1], xe_r.at[d - 1], d).start()
-    for d in range(1, tp):
-        tp_copy(xm_in, xm.at[me_tp], xm_s.at[d - 1], xm_r.at[d - 1], d).start()
+    xm_load = pltpu.make_async_copy(xm_in, xm.at[me_tp], w_sem.at[5])
+    xm_load.start()
+    xm_load.wait()
+    send(*mixer_part())
 
     loads = [
         pltpu.make_async_copy(h, v, w_sem.at[i])
@@ -127,52 +173,52 @@
     for load in loads:
         load.start()
 
-    xe[me_tp] = xe_in[...]
-    xm[me_tp] = xm_in[...]
-
-    def norm_into(gathered, gain):
-        def step(i, carry):
-            at = pl.ds(pl.multiple_of(i * chunk, chunk), chunk)
-            parts = [gathered[p, at, :].astype(f32) for p in range(tp)]
-            total = sum(jnp.sum(v, axis=-1, keepdims=True) for v in parts)
-            mean = total / width
-            parts = [v - mean for v in parts]
-            spread = sum(jnp.sum(v * v, axis=-1, keepdims=True) for v in parts) / width
-            inv = lax.rsqrt(spread + norm_eps)
-            for p in range(tp):
-                cols = slice(p * feat, (p + 1) * feat)
-                normed[at, cols] = (parts[p] * inv * gain[:, cols]).astype(bf16)
-            return carry
-
-        lax.fori_loop(0, rows // chunk, step, 0)
-
-    for d in range(1, tp):
-        tp_copy(xe_in, xe.at[tp_from(d)], xe_s.at[d - 1], xe_r.at[d - 1], d).wait_recv()
-    norm_into(xe, gain_e)
-
     def picked_rows(e):
         slot = lax.broadcasted_iota(jnp.int32, (cap, rows), 0) + e * cap
         hit = (slot == trow[0:1, :]) | (slot == trow[1:2, :])
         pick = jnp.where(hit, 1.0, 0.0).astype(bf16)
-        return jnp.dot(pick, normed[...], preferred_element_type=f32).astype(bf16)
+        return jnp.dot(pick, xe_in[...], preferred_element_type=f32).astype(bf16)
 
     def send_rows(d, carry):
         e = lax.rem(me_ep + d, ep)
         disp_send[e] = picked_rows(e)
-        ep_copy(disp_send.at[e], disp_recv.at[me_ep], dp_s.at[d], dp_r.at[d], d).start()
+        ep_copy(disp_send.at[e], slots.at[me_ep, me_tp], dp_s.at[d], dp_r.at[d], d).start()
         return carry
 
     lax.fori_loop(1, ep, send_rows, 0)
-    disp_recv[me_ep] = picked_rows(me_ep)
-
-    for d in range(1, tp):
-        tp_copy(xm_in, xm.at[tp_from(d)], xm_s.at[d - 1], xm_r.at[d - 1], d).wait_recv()
-    norm_into(xm, gain_m)
+    slots[me_ep, me_tp] = picked_rows(me_ep)
+    send(*slot_part(0))
+    relay(*mixer_part(), 0)
+
+    def pass_slots(k, carry):
+        q = ep_from(k)
+        ep_copy(disp_send.at[q], slots.at[q, me_tp], dp_s.at[k], dp_r.at[k], k).wait_recv()
+        send(*slot_part(k))
+        relay(*slot_part(k - 1), lax.rem(k, 2))
+        return carry
+
+    early = ep // 2
+    lax.fori_loop(1, early, pass_slots, 0)
+
+    def norm_rows(parts, gain):
+        parts = [v.astype(f32) for v in parts]
+        mean = sum(jnp.sum(v, axis=-1, keepdims=True) for v in parts) / width
+        parts = [v - mean for v in parts]
+        spread = sum(jnp.sum(v * v, axis=-1, keepdims=True) for v in parts) / width
+        inv = lax.rsqrt(spread + norm_eps)
+        return [
+            (v * inv * gain[:, p * feat : (p + 1) * feat]).astype(bf16)
+            for p, v in enumerate(parts)
+        ]
+
+    finish(*mixer_part())
     loads[0].wait()
 
     def project(i, carry):
         at = pl.ds(pl.multiple_of(i * chunk, chunk), chunk)
-        inner = jnp.dot(normed[at, :], w_in[...], preferred_element_type=f32).astype(bf16)
+        for p, v in enumerate(norm_rows([xm[p, at, :] for p in range(tp)], gain_m)):
+            normed[:, p * feat : (p + 1) * feat] = v
+        inner = jnp.dot(normed[...], w_in[...], preferred_element_type=f32).astype(bf16)
         ext[pl.ds(pl.multiple_of(RIM + i * chunk, RIM), chunk), :] = inner.astype(f32)
         return carry
 
@@ -184,16 +230,8 @@
     up_rim.start()
     down_rim.start()
 
-    loads[1].wait()
-    loads[2].wait()
-
-    def hidden_of(q):
-        x = disp_recv[q]
-        g = jnp.dot(x, gate[...], preferred_element_type=f32)
-        u = jnp.dot(x, up[...], preferred_element_type=f32)
-        return (g / (1.0 + jnp.exp(-g)) * u).astype(bf16)
-
-    hid[me_ep, me_tp] = hidden_of(me_ep)
+    lax.fori_loop(early, ep, pass_slots, 0)
+    relay(*slot_part(ep - 1), ep % 2)
 
     up_rim.wait_recv()
     down_rim.wait_recv()
@@ -225,31 +263,48 @@
         pooled[me_tp, i * chunk : (i + 1) * chunk, :] = (
             (result - values) * scale[...]
         ).astype(bf16)
-    for d in range(1, tp):
-        tp_copy(pooled.at[me_tp], pooled.at[me_tp], po_s.at[d - 1], po_r.at[d - 1], d).start()
-
-    def send_hidden(q, k):
-        for d in range(1, tp):
-            tp_copy(
-                hid.at[q, me_tp], hid.at[q, me_tp], hi_s.at[k, d - 1], hi_r.at[k, d - 1], d
-            ).start()
-
-    send_hidden(me_ep, 0)
-
-    def expert(k, carry):
-        q = ep_from(k)
-        ep_copy(disp_send.at[q], disp_recv.at[q], dp_s.at[k], dp_r.at[k], k).wait_recv()
-        hid[q, me_tp] = hidden_of(q)
-        send_hidden(q, k)
-        return carry
-
-    lax.fori_loop(1, ep, expert, 0)
+    send(*pooled_part())
+
+    loads[1].wait()
+    loads[2].wait()
+
+    def hidden_step(k):
+        q = ep_from(k)
+        finish(*slot_part(k))
+        for p, v in enumerate(norm_rows([slots[q, p] for p in range(tp)], gain_e)):
+            block[:, p * feat : (p + 1) * feat] = v
+        x = block[...]
+        g = jnp.dot(x, gate[...], preferred_element_type=f32)
+        u = jnp.dot(x, up[...], preferred_element_type=f32)
+        hid[q, me_tp] = (g / (1.0 + jnp.exp(-g)) * u).astype(bf16)
+        send(*hidden_part(k))
+
+    units = hid.shape[3]
+
+    def value_step(k):
+        q = ep_from(k)
+        finish(*hidden_part(k))
+        total = jnp.zeros((cap, out_e.shape[1]), f32)
+        for p in range(tp):
+            total = total + jnp.dot(
+                hid[q, p],
+                down[p * units : (p + 1) * units, :],
+                preferred_element_type=f32,
+            )
+        return total.astype(bf16)
+
+    def send_value(k):
+        q = ep_from(k)
+        back_send[q] = value_step(k)
+        ep_copy(back_send.at[q], back_recv.at[me_ep], bk_s.at[k], bk_r.at[k], ep - k).start()
+
+    hidden_step(0)
+    relay(*pooled_part(), 1)
+    hidden_step(1)
+    relay(*hidden_part(0), 1)
 
     loads[3].wait()
-    for d in range(1, tp):
-        tp_copy(
-            pooled.at[me_tp], pooled.at[tp_from(d)], po_s.at[d - 1], po_r.at[d - 1], d
-        ).wait_recv()
+    finish(*pooled_part())
 
     def mix_out(i, carry):
         at = pl.ds(pl.multiple_of(i * chunk, chunk), chunk)
@@ -265,33 +320,21 @@
 
     lax.fori_loop(0, rows // chunk, mix_out, 0)
     loads[4].wait()
-    units = hid.shape[3]
-
-    def value_of(q, k):
-        for d in range(1, tp):
-            tp_copy(
-                hid.at[q, me_tp], hid.at[q, tp_from(d)], hi_s.at[k, d - 1], hi_r.at[k, d - 1], d
-            ).wait_recv()
-        total = jnp.zeros((cap, out_e.shape[1]), f32)
-        for p in range(tp):
-            total = total + jnp.dot(
-                hid[q, p],
-                down[p * units : (p + 1) * units, :],
-                preferred_element_type=f32,
-            )
-        return total.astype(bf16)
-
-    back_recv[me_ep] = value_of(me_ep, 0)
-
-    def send_value(k, carry):
-        q = ep_from(k)
-        back_send[q] = value_of(q, k)
-        ep_copy(
-            back_send.at[q], back_recv.at[me_ep], bk_s.at[k], bk_r.at[k], ep - k
-        ).start()
-        return carry
-
-    lax.fori_loop(1, ep, send_value, 0)
+
+    hidden_step(2)
+    relay(*hidden_part(1), 0)
+    back_recv[me_ep] = value_step(0)
+
+    def expert(k, carry):
+        hidden_step(k)
+        relay(*hidden_part(k - 1), lax.rem(k, 2))
+        send_value(k - 2)
+        return carry
+
+    lax.fori_loop(3, ep, expert, 0)
+    relay(*hidden_part(ep - 1), ep % 2)
+    send_value(ep - 2)
+    send_value(ep - 1)
 
     def combine(e):
         slot = lax.broadcasted_iota(jnp.int32, (rows, cap), 1) + e * cap
@@ -316,33 +359,26 @@
     lax.fori_loop(1, ep, gather_value, 0)
     out_e[...] = acc[...].astype(bf16)
 
-    for d in range(1, tp):
-        tp_copy(xe_in, xe.at[me_tp], xe_s.at[d - 1], xe_r.at[d - 1], d).wait_send()
-        tp_copy(xm_in, xm.at[me_tp], xm_s.at[d - 1], xm_r.at[d - 1], d).wait_send()
-        tp_copy(
-            pooled.at[me_tp], pooled.at[me_tp], po_s.at[d - 1], po_r.at[d - 1], d
-        ).wait_send()
+    drain(*mixer_part())
+    drain(*pooled_part())
     up_rim.wait_send()
     down_rim.wait_send()
 
-    def drain(k, carry):
+    def drain_ep(k, carry):
         e = lax.rem(me_ep + k, ep)
         q = ep_from(k)
-        ep_copy(disp_send.at[e], disp_recv.at[me_ep], dp_s.at[k], dp_r.at[k], k).wait_send()
+        ep_copy(disp_send.at[e], slots.at[me_ep, me_tp], dp_s.at[k], dp_r.at[k], k).wait_send()
         ep_copy(back_send.at[q], back_recv.at[me_ep], bk_s.at[k], bk_r.at[k], ep - k).wait_send()
         return carry
 
-    lax.fori_loop(1, ep, drain, 0)
-
-    def drain_hidden(k, carry):
-        q = ep_from(k)
-        for d in range(1, tp):
-            tp_copy(
-                hid.at[q, me_tp], hid.at[q, me_tp], hi_s.at[k, d - 1], hi_r.at[k, d - 1], d
-            ).wait_send()
-        return carry
-
-    lax.fori_loop(0, ep, drain_hidden, 0)
+    lax.fori_loop(1, ep, drain_ep, 0)
+
+    def drain_tp(k, carry):
+        drain(*slot_part(k))
+        drain(*hidden_part(k))
+        return carry
+
+    lax.fori_loop(0, ep, drain_tp, 0)
 
 
 def on_device(
@@ -390,10 +426,10 @@
             pltpu.VMEM(expert_up.shape[1:], bf16),
             pltpu.VMEM(expert_down.shape[1:], bf16),
             pltpu.VMEM((tp, rows, feat), bf16),
-            pltpu.VMEM((tp, rows, feat), bf16),
-            pltpu.VMEM((rows, width), bf16),
-            pltpu.VMEM((ep, cap, width), bf16),
-            pltpu.VMEM((ep, cap, width), bf16),
+            pltpu.VMEM((min(rows, 128), width), bf16),
+            pltpu.VMEM((cap, width), bf16),
+            pltpu.VMEM((ep, cap, feat), bf16),
+            pltpu.VMEM((ep, tp, cap, feat), bf16),
             pltpu.VMEM((ep, tp, cap, units), bf16),
             pltpu.VMEM((tp, rows, chan), bf16),
             pltpu.VMEM((ep, cap, expert_down.shape[2]), bf16),
@@ -402,9 +438,9 @@
             pltpu.VMEM((2, RIM, chan), bf16),
             pltpu.VMEM((2, RIM, chan), bf16),
             pltpu.VMEM((rows, expert_down.shape[2]), f32),
-            dma((5,)),
-            dma((tp - 1,)),
-            dma((tp - 1,)),
+            dma((6,)),
+            dma((ep, tp - 1)),
+            dma((ep, tp - 1)),
             dma((tp - 1,)),
             dma((tp - 1,)),
             dma((ep,)),

time: 251 us -> 181 us (0.72)
  Pallas kernels: 238 us -> 170 us
    pallas_call x1, Pallas kernels: 238 us -> 170 us  [on_device(): pl.pallas_call(functools.partial(fused, ep, tp), out_shape=(jax.ShapeDtyp...]
where the time goes in v2:
time: 181 us
  Pallas kernels  170 us (94%)
  local copies, waits for them, and re-layouts  7.1 us (4%)
  other arithmetic  3.26 us (2%)
    pallas_call x1, Pallas kernels, on_device(): pl.pallas_call(functools.partial(fused, ep, tp), out_shape=(jax.ShapeDtyp...  170 us
    unnamed x8, local copies, waits for them, and re-layouts  5.44 us

profile of v2, /device:TPU:0, one launch (start us, length us, event | category | flops | bytes accessed | tf_op | source)
XLA Modules:
  0.0 181.0 jit_solution(3560070372970018279)
XLA Ops:
  0.6 0.0 copy-start.1
  0.6 0.7 broadcast_multiply_fusion
  1.3 0.1 copy.26
  1.5 0.8 copy.24
  2.3 0.2 eq.29
  2.5 0.2 eq.25
  2.7 2.3 %reduce-window.6 = s32[8,8,128]{2,1,0:T(8,128)S(1)} reduce-window(s32[8,8,128]{2,1,0:T(8,128)S(1)} %fusion.2, s32[]{:T(128)} %constant.9.clone.1), window={size=1x1x128 pad=0_0x0_0x127_0}, to_apply=%region_0.0 | reduce-window | flops 1040384 | bytes 65540 | tf_op jit(solution)/shard_map/reduce-window
  5.0 0.3 slice_reduce_fusion
  5.2 0.2 reduce-window.9
  5.4 0.1 add_bitcast_fusion
  5.5 0.2 reduce_sum.12
  5.7 0.0 copy-start
  5.8 0.7 copy.27.trow
  6.5 0.0 copy-done.1
  6.5 0.9 copy.28.rw
  7.3 0.0 copy-done
  7.3 169.9 %shard_map.131 = (bf16[512,512]{1,0:T(8,128)(2,1)}, bf16[512,512]{1,0:T(8,128)(2,1)}) custom-call(bf16[512,512]{1,0:T(8,128)(2,1)} %xm_in.1, bf16[512,512]{1,0:T(8,128)(2,1)} %xe_in.1, f32[1,2048]{1,0:T(1,128)} %bitcast.27, f32[1,2048]{1,0:T(1,128)} %bitcast.28, f32[1,512]{1,0:T(1,128)} %bitcast.29, s32[2,512]{1,0:T(2,128)} %copy.27.trow, s32[512,2]{1,0:T(8,128)} %copy-done, ...), custom_call_target="tpu_custom_call" | custom-call | tf_op jit(solution)/shard_map/pallas_call | solution.py:414
  177.3 1.9 %copy.33 = bf16[512,512]{1,0:T(8,128)(2,1)} copy(bf16[512,512]{1,0:T(8,128)(2,1)} %get-tuple-element.4) | data formatting | bytes 1048576
  179.1 1.9 %copy.34 = bf16[512,512]{1,0:T(8,128)(2,1)} copy(bf16[512,512]{1,0:T(8,128)(2,1)} %get-tuple-element.5) | data formatting | bytes 1048576
  (3 shorter events, 0.1 us)
Async XLA Ops:
  0.6 5.8 %copy-start.1 = (f32[512,2]{0,1:T(2,128)S(1)}, f32[512,2]{0,1:T(2,128)}, u32[]{:S(2)}) copy-start(f32[512,2]{0,1:T(2,128)} %param.23) | copy-start | bytes 12292
  5.7 1.6 copy-start

commit v3 on v2

--- a/solution.py
+++ b/solution.py
@@ -24,8 +24,8 @@
     gain_m,
     gain_e,
     scale,
-    trow,
-    tcol,
+    route_rows,
+    route_cols,
     rw,
     w_in_h,
     w_mix_h,
@@ -52,6 +52,7 @@
     rim_send,
     rim_recv,
     acc,
+    tcol,
     w_sem,
     sl_s,
     sl_r,
@@ -173,9 +174,35 @@
     for load in loads:
         load.start()
 
+    t0 = lax.broadcasted_iota(jnp.int32, (rows, rows), 0)
+    t1 = lax.broadcasted_iota(jnp.int32, (rows, rows), 1)
+    names = lax.broadcasted_iota(jnp.int32, (ep, rows), 0)
+    named = [jnp.where(route_rows[j : j + 1, :] == names, 1.0, 0.0) for j in range(TOP)]
+    ahead = jnp.dot(
+        sum(named).astype(bf16),
+        jnp.where(t0 < t1, 1.0, 0.0).astype(bf16),
+        preferred_element_type=f32,
+    )
+    trow = [
+        route_rows[j : j + 1, :] * cap
+        + jnp.sum(named[j] * ahead, axis=0, keepdims=True).astype(jnp.int32)
+        for j in range(TOP)
+    ]
+    names = lax.broadcasted_iota(jnp.int32, (rows, ep), 1)
+    named = [jnp.where(route_cols[:, j : j + 1] == names, 1.0, 0.0) for j in range(TOP)]
+    ahead = jnp.dot(
+        jnp.where(t1 < t0, 1.0, 0.0).astype(bf16),
+        sum(named).astype(bf16),
+        preferred_element_type=f32,
+    )
+    for j in range(TOP):
+        tcol[:, j : j + 1] = route_cols[:, j : j + 1] * cap + jnp.sum(
+            named[j] * ahead, axis=1, keepdims=True
+        ).astype(jnp.int32)
+
     def picked_rows(e):
         slot = lax.broadcasted_iota(jnp.int32, (cap, rows), 0) + e * cap
-        hit = (slot == trow[0:1, :]) | (slot == trow[1:2, :])
+        hit = (slot == trow[0]) | (slot == trow[1])
         pick = jnp.where(hit, 1.0, 0.0).astype(bf16)
         return jnp.dot(pick, xe_in[...], preferred_element_type=f32).astype(bf16)
 
@@ -187,18 +214,22 @@
 
     lax.fori_loop(1, ep, send_rows, 0)
     slots[me_ep, me_tp] = picked_rows(me_ep)
-    send(*slot_part(0))
     relay(*mixer_part(), 0)
 
-    def pass_slots(k, carry):
+    def arrive(k):
         q = ep_from(k)
         ep_copy(disp_send.at[q], slots.at[q, me_tp], dp_s.at[k], dp_r.at[k], k).wait_recv()
         send(*slot_part(k))
+
+    arrive(1)
+
+    def pass_slots(k, carry):
+        arrive(k)
         relay(*slot_part(k - 1), lax.rem(k, 2))
         return carry
 
     early = ep // 2
-    lax.fori_loop(1, early, pass_slots, 0)
+    lax.fori_loop(2, early, pass_slots, 0)
 
     def norm_rows(parts, gain):
         parts = [v.astype(f32) for v in parts]
@@ -230,8 +261,7 @@
     up_rim.start()
     down_rim.start()
 
-    lax.fori_loop(early, ep, pass_slots, 0)
-    relay(*slot_part(ep - 1), ep % 2)
+    lax.fori_loop(early, ep - 1, pass_slots, 0)
 
     up_rim.wait_recv()
     down_rim.wait_recv()
@@ -264,6 +294,8 @@
             (result - values) * scale[...]
         ).astype(bf16)
     send(*pooled_part())
+    pass_slots(ep - 1, 0)
+    send(*slot_part(0))
 
     loads[1].wait()
     loads[2].wait()
@@ -298,10 +330,12 @@
         back_send[q] = value_step(k)
         ep_copy(back_send.at[q], back_recv.at[me_ep], bk_s.at[k], bk_r.at[k], ep - k).start()
 
-    hidden_step(0)
+    hidden_step(1)
+    relay(*slot_part(ep - 1), ep % 2)
+    hidden_step(2)
+    relay(*slot_part(0), 1 - ep % 2)
     relay(*pooled_part(), 1)
-    hidden_step(1)
-    relay(*hidden_part(0), 1)
+    relay(*hidden_part(1), 0)
 
     loads[3].wait()
     finish(*pooled_part())
@@ -321,10 +355,6 @@
     lax.fori_loop(0, rows // chunk, mix_out, 0)
     loads[4].wait()
 
-    hidden_step(2)
-    relay(*hidden_part(1), 0)
-    back_recv[me_ep] = value_step(0)
-
     def expert(k, carry):
         hidden_step(k)
         relay(*hidden_part(k - 1), lax.rem(k, 2))
@@ -332,9 +362,12 @@
         return carry
 
     lax.fori_loop(3, ep, expert, 0)
+    hidden_step(0)
     relay(*hidden_part(ep - 1), ep % 2)
     send_value(ep - 2)
+    relay(*hidden_part(0), 1 - ep % 2)
     send_value(ep - 1)
+    back_recv[me_ep] = value_step(0)
 
     def combine(e):
         slot = lax.broadcasted_iota(jnp.int32, (rows, cap), 1) + e * cap
@@ -403,11 +436,6 @@
     cap = (3 * TOP * rows + 2 * ep - 1) // (2 * ep)
     chan = w_in.shape[1]
     units = expert_gate.shape[2]
-    flat_route = routes.reshape(-1)
-    onehot = (flat_route[:, None] == jnp.arange(ep, dtype=jnp.int32)[None, :]).astype(jnp.int32)
-    ranking = jnp.sum(onehot * (jnp.cumsum(onehot, axis=0) - 1), axis=1)
-    target = (flat_route * cap + ranking).reshape(rows, TOP)
-
     vmem = pl.BlockSpec(memory_space=pltpu.VMEM)
     hbm = pl.BlockSpec(memory_space=pl.ANY)
     dma = pltpu.SemaphoreType.DMA
@@ -438,6 +466,7 @@
             pltpu.VMEM((2, RIM, chan), bf16),
             pltpu.VMEM((2, RIM, chan), bf16),
             pltpu.VMEM((rows, expert_down.shape[2]), f32),
+            pltpu.VMEM((rows, TOP), jnp.int32),
             dma((6,)),
             dma((ep, tp - 1)),
             dma((ep, tp - 1)),
@@ -463,8 +492,8 @@
         mixer_gain.reshape(1, width),
         expert_gain.reshape(1, width),
         pool_scale.reshape(1, chan),
-        target.T,
-        target,
+        routes.T,
+        routes,
         route_weight,
         w_in,
         w_mix_out,

time: 181 us -> 176 us (0.972)
  other arithmetic: 3.26 us -> 0 us
    another operation x2 -> x0, other arithmetic: 2.43 us -> none
    unnamed x8 -> x4, local copies, waits for them, and re-layouts: 5.44 us -> 6.82 us
where the time goes in v3:
time: 176 us
  Pallas kernels  169 us (96%)
  local copies, waits for them, and re-layouts  6.82 us (4%)
    pallas_call x1, Pallas kernels, on_device(): pl.pallas_call(functools.partial(fused, ep, tp), out_shape=(jax.ShapeDtyp...  169 us
    unnamed x4, local copies, waits for them, and re-layouts  6.82 us

profile of v3, /device:TPU:0, one launch (start us, length us, event | category | flops | bytes accessed | tf_op | source)
XLA Modules:
  0.0 176.0 jit_solution(6231510909672208844)
XLA Ops:
  0.6 1.5 copy.15.rw
  2.2 1.5 copy.14.route_cols
  3.7 168.6 %shard_map.131 = (bf16[512,512]{1,0:T(8,128)(2,1)}, bf16[512,512]{1,0:T(8,128)(2,1)}) custom-call(bf16[512,512]{1,0:T(8,128)(2,1)} %xm_in.1, bf16[512,512]{1,0:T(8,128)(2,1)} %xe_in.1, f32[1,2048]{1,0:T(1,128)} %bitcast.11, f32[1,2048]{1,0:T(1,128)} %bitcast.12, f32[1,512]{1,0:T(1,128)} %bitcast.13, s32[2,512]{1,0:T(2,128)} %bitcast.10, ...), custom_call_target="tpu_custom_call" | custom-call | tf_op jit(solution)/shard_map/pallas_call | solution.py:442
  172.3 1.9 %copy.18 = bf16[512,512]{1,0:T(8,128)(2,1)} copy(bf16[512,512]{1,0:T(8,128)(2,1)} %get-tuple-element.4) | data formatting | bytes 1048576
  174.1 1.9 %copy.19 = bf16[512,512]{1,0:T(8,128)(2,1)} copy(bf16[512,512]{1,0:T(8,128)(2,1)} %get-tuple-element.5) | data formatting | bytes 1048576

commit v4 on v3

--- a/solution.py
+++ b/solution.py
@@ -25,8 +25,7 @@
     gain_e,
     scale,
     route_rows,
-    route_cols,
-    rw,
+    rw_rows,
     w_in_h,
     w_mix_h,
     gate_h,
@@ -52,7 +51,8 @@
     rim_send,
     rim_recv,
     acc,
-    tcol,
+    as_rows,
+    as_cols,
     w_sem,
     sl_s,
     sl_r,
@@ -188,17 +188,11 @@
         + jnp.sum(named[j] * ahead, axis=0, keepdims=True).astype(jnp.int32)
         for j in range(TOP)
     ]
-    names = lax.broadcasted_iota(jnp.int32, (rows, ep), 1)
-    named = [jnp.where(route_cols[:, j : j + 1] == names, 1.0, 0.0) for j in range(TOP)]
-    ahead = jnp.dot(
-        jnp.where(t1 < t0, 1.0, 0.0).astype(bf16),
-        sum(named).astype(bf16),
-        preferred_element_type=f32,
-    )
+    as_rows[...] = jnp.zeros_like(as_rows)
     for j in range(TOP):
-        tcol[:, j : j + 1] = route_cols[:, j : j + 1] * cap + jnp.sum(
-            named[j] * ahead, axis=1, keepdims=True
-        ).astype(jnp.int32)
+        as_rows[j : j + 1, :] = trow[j].astype(f32)
+        as_rows[TOP + j : TOP + j + 1, :] = rw_rows[j : j + 1, :]
+    as_cols[...] = as_rows[...].T
 
     def picked_rows(e):
         slot = lax.broadcasted_iota(jnp.int32, (cap, rows), 0) + e * cap
@@ -367,13 +361,13 @@
     send_value(ep - 2)
     relay(*hidden_part(0), 1 - ep % 2)
     send_value(ep - 1)
-    back_recv[me_ep] = value_step(0)
 
     def combine(e):
         slot = lax.broadcasted_iota(jnp.int32, (rows, cap), 1) + e * cap
-        weight = jnp.where(slot == tcol[:, 0:1], rw[:, 0:1], 0.0) + jnp.where(
-            slot == tcol[:, 1:2], rw[:, 1:2], 0.0
-        )
+        weight = jnp.zeros((rows, cap), f32)
+        for j in range(TOP):
+            own_slot = as_cols[:, j : j + 1].astype(jnp.int32)
+            weight = weight + jnp.where(slot == own_slot, as_cols[:, TOP + j : TOP + j + 1], 0.0)
         coarse = weight.astype(bf16)
         fine = (weight - coarse.astype(f32)).astype(bf16)
         v = back_recv[e]
@@ -381,7 +375,7 @@
             fine, v, preferred_element_type=f32
         )
 
-    acc[...] = combine(me_ep)
+    acc[...] = jnp.zeros_like(acc)
 
     def gather_value(k, carry):
         e = lax.rem(me_ep + k, ep)
@@ -389,7 +383,10 @@
         acc[...] += combine(e)
         return carry
 
-    lax.fori_loop(1, ep, gather_value, 0)
+    lax.fori_loop(1, ep - 2, gather_value, 0)
+    back_recv[me_ep] = value_step(0)
+    acc[...] += combine(me_ep)
+    lax.fori_loop(ep - 2, ep, gather_value, 0)
     out_e[...] = acc[...].astype(bf16)
 
     drain(*mixer_part())
@@ -445,7 +442,7 @@
             jax.ShapeDtypeStruct((rows, w_mix_out.shape[1]), bf16),
             jax.ShapeDtypeStruct((rows, expert_down.shape[2]), bf16),
         ),
-        in_specs=[vmem] * 8 + [hbm] * 5,
+        in_specs=[vmem] * 7 + [hbm] * 5,
         out_specs=(vmem, vmem),
         scratch_shapes=[
             pltpu.VMEM(w_in.shape, bf16),
@@ -466,7 +463,8 @@
             pltpu.VMEM((2, RIM, chan), bf16),
             pltpu.VMEM((2, RIM, chan), bf16),
             pltpu.VMEM((rows, expert_down.shape[2]), f32),
-            pltpu.VMEM((rows, TOP), jnp.int32),
+            pltpu.VMEM((8, rows), f32),
+            pltpu.VMEM((rows, 8), f32),
             dma((6,)),
             dma((ep, tp - 1)),
             dma((ep, tp - 1)),
@@ -493,8 +491,7 @@
         expert_gain.reshape(1, width),
         pool_scale.reshape(1, chan),
         routes.T,
-        routes,
-        route_weight,
+        route_weight.T,
         w_in,
         w_mix_out,
         expert_gate.reshape(expert_gate.shape[1:]),

time: 176 us -> 171 us (0.972)
  local copies, waits for them, and re-layouts: 6.82 us -> 3.74 us
  Pallas kernels: 169 us -> 166 us
    unnamed x4 -> x2, local copies, waits for them, and re-layouts: 6.82 us -> 3.74 us
    pallas_call x1, Pallas kernels: 169 us -> 166 us  [on_device(): pl.pallas_call(functools.partial(fused, ep, tp), out_shape=(jax.ShapeDtyp...]
where the time goes in v4:
time: 171 us
  Pallas kernels  166 us (97%)
  local copies, waits for them, and re-layouts  3.74 us (2%)
    pallas_call x1, Pallas kernels, on_device(): pl.pallas_call(functools.partial(fused, ep, tp), out_shape=(jax.ShapeDtyp...  166 us
    unnamed x2, local copies, waits for them, and re-layouts  3.74 us

profile of v4, /device:TPU:0, one launch (start us, length us, event | category | flops | bytes accessed | tf_op | source)
XLA Modules:
  0.0 170.5 jit_solution(731890658768766045)
XLA Ops:
  0.6 166.2 %shard_map.131 = (bf16[512,512]{1,0:T(8,128)(2,1)}, bf16[512,512]{1,0:T(8,128)(2,1)}) custom-call(bf16[512,512]{1,0:T(8,128)(2,1)} %xm_in.1, bf16[512,512]{1,0:T(8,128)(2,1)} %xe_in.1, f32[1,2048]{1,0:T(1,128)} %bitcast.11, f32[1,2048]{1,0:T(1,128)} %bitcast.12, f32[1,512]{1,0:T(1,128)} %bitcast.15, s32[2,512]{1,0:T(2,128)} %bitcast.13, f32[2,512]{1,0:T(2,128)} %bitcast.14, ...), custom_call_target="tpu_custom_call" | custom-call | tf_op jit(solution)/shard_map/pallas_call | solution.py:439
  166.8 1.9 %copy.16 = bf16[512,512]{1,0:T(8,128)(2,1)} copy(bf16[512,512]{1,0:T(8,128)(2,1)} %get-tuple-element.4) | data formatting | bytes 1048576
  168.7 1.9 %copy.17 = bf16[512,512]{1,0:T(8,128)(2,1)} copy(bf16[512,512]{1,0:T(8,128)(2,1)} %get-tuple-element.5) | data formatting | bytes 1048576
